TPU v7x, 512 devices: a 8x2x16 block of a 8x16x16 slice. The times are simulated.
512 devices in a mesh: grp: 2 (over y), ra: 16 (over z), cb: 16 (over x, core).
Axes of the slice: x: 8, y: 2, z: 16, core: 2. Of those that a mesh axis runs over, the one named last changes fastest.
The devices are a block of a 8x16x16 slice.
Arguments:
- residual: bfloat16 [512, 4096], P('grp', 'ra'), parts along dimension 0, may hold values from -6 to 6
- gain_first: bfloat16 [4096], P('ra'), may hold values from 0.099609375 to 1.8984375
- gate_first: bfloat16 [4096, 11264], P('ra', 'cb'), may hold values from -0.09375 to 0.09375
- up_first: bfloat16 [4096, 11264], P('ra', 'cb'), may hold values from -0.09375 to 0.09375
- down_first: bfloat16 [11264, 4096], P('cb', 'ra'), may hold values from -0.078125 to 0.078125
- gain_second: bfloat16 [4096], P('ra'), may hold values from 0.099609375 to 1.8984375
- gate_second: bfloat16 [4096, 11264], P('ra', 'cb'), may hold values from -0.09375 to 0.09375
- up_second: bfloat16 [4096, 11264], P('ra', 'cb'), may hold values from -0.09375 to 0.09375
- down_second: bfloat16 [11264, 4096], P('cb', 'ra'), may hold values from -0.078125 to 0.078125
Outputs:
- updated: bfloat16 [512, 4096], P('grp', 'ra'), parts along dimension 0
There are 2 independent parts, one for each index of `grp`. A program takes and returns all parts, laid end to end along the dimension named above; an argument that names none is the same for every part. Nothing has to cross between parts.
All inputs are finite; a program needn't handle non-finite values.
Results may differ from a plain program's by a relative error of at most 0.0071.
Values may be sent and summed in bfloat16 or wider, within the bound.
No kernel may reach another device: no remote copies, remote signals or barrier semaphores. Data moves between devices by JAX's collectives and lax.ppermute only.
A program may use at most 64 MiB of HBM per device.

v0:
```python
import jax
import jax.numpy as jnp
from jax import lax
from jax.sharding import PartitionSpec as P

D = 4096


epsilon = 1e-06


def in_one_piece(arrays, axis, dim, along):
    widths = [a.shape[along] for a in arrays]
    both = jnp.concatenate(arrays, axis=along)
    out = lax.psum_scatter(both, axis, scatter_dimension=dim, tiled=True)
    return tuple(jnp.split(out, [sum(widths[:k]) for k in range(1, len(widths))], axis=along))


def sent_to_all(array, axis):
    peers = lax.axis_size(axis)
    return lax.all_to_all(
        jnp.broadcast_to(array[None], (peers, *array.shape)), axis, 0, 0, tiled=True
    )


def joined_along(tiles, dim):
    tiles = jnp.moveaxis(tiles, 0, dim)
    shape = tiles.shape
    return tiles.reshape(*shape[:dim], shape[dim] * shape[dim + 1], *shape[dim + 2 :])


def gather_directly(array, axis, dim):
    tiles = sent_to_all(array, axis)
    return joined_along(tiles, dim)


def total_of_pieces(array, axis):
    return lax.all_gather(array, axis).sum(0)


def half_step(stream, gain, w_gate, w_up, w_down):
    values = stream.astype(jnp.float32)
    square_part = jnp.sum(values * values, axis=1, keepdims=True)
    normed = (values * gain.astype(jnp.float32)).astype(jnp.bfloat16)
    gate_part = jnp.dot(normed, w_gate, preferred_element_type=jnp.float32)
    up_part = jnp.dot(normed, w_up, preferred_element_type=jnp.float32)
    gate_sum, up_sum, square_sum = in_one_piece((gate_part, up_part, square_part), "ra", 0, 1)
    scale = lax.rsqrt(square_sum / D + epsilon)
    hidden = (jax.nn.silu(scale * gate_sum) * (scale * up_sum)).astype(jnp.bfloat16)
    down_part = jnp.dot(
        gather_directly(hidden, "ra", 0), w_down, preferred_element_type=jnp.float32
    )
    branch = total_of_pieces(down_part, "cb")
    return (values + 0.5 * branch).astype(jnp.bfloat16)


def per_device(
    residual,
    gain_first,
    gate_first,
    up_first,
    down_first,
    gain_second,
    gate_second,
    up_second,
    down_second,
):
    middle = half_step(residual, gain_first, gate_first, up_first, down_first)
    return half_step(middle, gain_second, gate_second, up_second, down_second)


def solution(mesh):
    in_specs = (
        P("grp", "ra"),
        P("ra"),
        P("ra", "cb"),
        P("ra", "cb"),
        P("cb", "ra"),
        P("ra"),
        P("ra", "cb"),
        P("ra", "cb"),
        P("cb", "ra"),
    )
    out_specs = P("grp", "ra")
    return jax.shard_map(
        per_device, mesh=mesh, in_specs=in_specs, out_specs=out_specs, check_vma=False
    )
```

profile of v0, /device:TPU:65, one launch (start us, length us, event | category | flops | bytes accessed | tf_op | source)
XLA Modules:
  0.0 353.4 jit_solution(2841522730455635302)
XLA Ops:
  6.6 0.7 convert_element_type.31
  7.3 1.0 fusion.1
  8.3 1.2 fusion.10
  9.5 1.2 fusion.12
  10.7 0.1 pad_maximum_fusion
  10.8 1.6 copy.18
  12.5 0.1 all-gather.5.cloned.1.call-start
  12.6 99.2 %reduce-scatter.7.cloned.1.call-done = f32[16,1409]{1,0:T(8,128)} async-done(((f32[256,1409]{1,0:T(8,128)}), f32[16,1409]{1,0:T(8,128)}) %reduce-scatter.7.cloned.1.call-update) | async-done | bytes 90192 | tf_op jit(solution)/shard_map/reduce_scatter | solution.py:15
  111.8 0.7 add_rsqrt_fusion.1
  112.5 0.1 copy.24
  112.6 1.0 fusion.17
  113.6 22.3 %all_to_all.10 = bf16[16,16,704]{2,1,0:T(8,128)(2,1)S(1)} all-to-all(bf16[16,16,704]{2,1,0:T(8,128)(2,1)S(1)} %broadcast_in_dim.9), channel_id=1, replica_groups=mesh['grp'=2,'ra'=16,'cb'=16] {'ra'}, dimensions={0} | all-to-all | bytes 720896 | tf_op jit(solution)/shard_map/all_to_all | solution.py:21
  135.9 1.0 fusion.19
  137.0 0.1 reduce-scatter.9.cloned.1.call-start
  137.1 56.3 %all-gather.5.cloned.1.call-done = f32[4096,256]{1,0:T(8,128)} async-done(((f32[256,256]{1,0:T(8,128)}), f32[4096,256]{1,0:T(8,128)}) %all-gather.5.cloned.1.call-update) | async-done | bytes 4194320 | tf_op jit(solution)/shard_map/all_gather | solution.py:38
  193.3 2.5 reduce_sum.37
  195.9 0.1 fusion.4
  196.0 0.3 fusion.6
  196.3 0.6 copy-done.5
  196.9 0.3 fusion.8
  197.1 0.1 pad_maximum_fusion.1
  197.3 1.6 copy.20
  199.0 0.1 all-gather.7.cloned.1.call-start
  199.0 63.2 %reduce-scatter.9.cloned.1.call-done = f32[16,1409]{1,0:T(8,128)} async-done(((f32[256,1409]{1,0:T(8,128)}), f32[16,1409]{1,0:T(8,128)}) %reduce-scatter.9.cloned.1.call-update) | async-done | bytes 90192 | tf_op jit(solution)/shard_map/reduce_scatter | solution.py:15
  262.3 0.7 add_rsqrt_fusion
  263.0 0.1 copy.25
  263.1 1.0 fusion.15
  264.1 23.0 %all_to_all.11 = bf16[16,16,704]{2,1,0:T(8,128)(2,1)S(1)} all-to-all(bf16[16,16,704]{2,1,0:T(8,128)(2,1)S(1)} %broadcast_in_dim.11), channel_id=1, replica_groups=mesh['grp'=2,'ra'=16,'cb'=16] {'ra'}, dimensions={0} | all-to-all | bytes 720896 | tf_op jit(solution)/shard_map/all_to_all | solution.py:21
  287.0 1.0 fusion.20
  288.1 55.6 %all-gather.7.cloned.1.call-done = f32[4096,256]{1,0:T(8,128)} async-done(((f32[256,256]{1,0:T(8,128)}), f32[4096,256]{1,0:T(8,128)}) %all-gather.7.cloned.1.call-update) | async-done | bytes 4194320 | tf_op jit(solution)/shard_map/all_gather | solution.py:38
  343.7 2.5 reduce_sum.39
  346.1 0.7 fusion.5
  (23 shorter events, 0.3 us)
Async XLA Ops:
  6.5 1.8 copy-start
  6.6 3.0 copy-start.2
  6.6 105.2 %reduce-scatter.7.cloned.1.call-start = ((), (), s32[]{:S(2)}) async-start(), calls=%async_computation.6 | async-start | bytes 1671168 | tf_op jit(solution)/shard_map/reduce_scatter | solution.py:15
  12.5 123.5 %copy-start.3 = (bf16[704,256]{1,0:T(8,128)(2,1)S(1)}, bf16[704,256]{1,0:T(8,128)(2,1)}, u32[]{:S(2)}) copy-start(bf16[704,256]{1,0:T(8,128)(2,1)} %param.13) | copy-start | bytes 1081348
  12.5 124.5 %copy-start.7 = (bf16[256]{0:T(256)(128)(2,1)S(1)}, bf16[256]{0:T(256)(128)(2,1)}, u32[]{:S(2)}) copy-start(bf16[256]{0:T(256)(128)(2,1)} %param.14) | copy-start | bytes 1540
  12.5 180.8 %all-gather.5.cloned.1.call-start = ((), (), s32[]{:S(2)}) async-start(), calls=%async_computation.4 | async-start | bytes 4456448 | tf_op jit(solution)/shard_map/all_gather | solution.py:38
  137.0 125.3 %reduce-scatter.9.cloned.1.call-start = ((), (), s32[]{:S(2)}) async-start(), calls=%async_computation.7 | async-start | bytes 1671168 | tf_op jit(solution)/shard_map/reduce_scatter | solution.py:15
  193.3 2.5 copy-start.1
  193.3 2.7 copy-start.4
  195.9 1.0 copy-start.5
  198.9 88.1 %copy-start.6 = (bf16[704,256]{1,0:T(8,128)(2,1)S(1)}, bf16[704,256]{1,0:T(8,128)(2,1)}, u32[]{:S(2)}) copy-start(bf16[704,256]{1,0:T(8,128)(2,1)} %param.17) | copy-start | bytes 1081348
  199.0 144.7 %all-gather.7.cloned.1.call-start = ((), (), s32[]{:S(2)}) async-start(), calls=%async_computation.5 | async-start | bytes 4456448 | tf_op jit(solution)/shard_map/all_gather | solution.py:38
Sparse Core Ops, SparseCore 0:
  12.6 99.0 reduce-scatter.6
  137.1 56.1 all-gather.4
  199.1 63.1 reduce-scatter.8
  288.2 55.4 all-gather.6
where the time goes:
time: 354 us; the launch traced here: 353 us
  waiting for transfers between devices  274 us (77%)
  blocking collectives  45.3 us (13%)
  between operations  13.3 us (4%)
  other arithmetic  11.1 us (3%)
  matrix products  4.88 us (1%)
  local copies, waits for them, and re-layouts  4.08 us (1%)
    reduce_scatter x2, waiting for transfers between devices, in_one_piece(): out = lax.psum_scatter(both, axis, scatter_dimension=dim, tiled=True)  162 us
    all_gather x2, waiting for transfers between devices, total_of_pieces(): return lax.all_gather(array, axis).sum(0)  112 us
    all_to_all x2, blocking collectives, sent_to_all(): lax.all_to_all(jnp.broadcast_to(array[None], (peers, *array.shape)), axis...  45.3 us
  transfers between devices with their start and end apart: 4, of which 4 were waited for; matrix products, arithmetic and copies ran while one was open for 0% of the time, Pallas kernels for 0%

commit v1 on v0

v1 whole, which is shorter than its diff:
```python
import jax
import jax.numpy as jnp
from jax import lax
from jax.sharding import PartitionSpec as P

LANES = 128

epsilon = 1e-06


def exchanged(array, axis):
    return lax.all_to_all(array, axis, 0, 0, tiled=True)


def sent_to_all(array, axis):
    peers = lax.axis_size(axis)
    return exchanged(jnp.broadcast_to(array[None], (peers, *array.shape)), axis)


def in_two_halves(value):
    high = value.astype(jnp.bfloat16)
    low = (value - high.astype(jnp.float32)).astype(jnp.bfloat16)
    return high, low


def half_step(stream, gain, w_gate, w_up, w_down):
    width = stream.shape[1] * lax.axis_size("ra")
    tokens = stream.shape[0]
    units = w_gate.shape[1]
    ra, cb = lax.axis_size("ra"), lax.axis_size("cb")
    values = stream.astype(jnp.float32)
    square_part = jnp.sum(values * values, axis=1, keepdims=True)
    normed = (values * gain.astype(jnp.float32)).astype(jnp.bfloat16)
    gate_part = jnp.dot(normed, w_gate, preferred_element_type=jnp.float32)
    up_part = jnp.dot(normed, w_up, preferred_element_type=jnp.float32)
    high, low = in_two_halves(square_part)
    squares = jnp.concatenate([high, low, jnp.zeros((tokens, LANES - 2), jnp.bfloat16)], axis=1)
    parts = jnp.concatenate(
        [gate_part.astype(jnp.bfloat16), up_part.astype(jnp.bfloat16), squares], axis=1
    )
    parts = exchanged(parts.reshape(ra, tokens // ra, parts.shape[1]), "ra")
    total = jnp.sum(parts.astype(jnp.float32), axis=0)
    gate_sum, up_sum = total[:, :units], total[:, units : 2 * units]
    square_sum = total[:, 2 * units : 2 * units + 1] + total[:, 2 * units + 1 : 2 * units + 2]
    scale = lax.rsqrt(square_sum / width + epsilon)
    hidden = (jax.nn.silu(scale * gate_sum) * (scale * up_sum)).astype(jnp.bfloat16)
    hidden = sent_to_all(hidden, "ra").reshape(tokens, units)
    down_part = jnp.dot(hidden, w_down, preferred_element_type=jnp.float32)
    pieces = exchanged(
        down_part.astype(jnp.bfloat16).reshape(cb, tokens // cb, stream.shape[1]), "cb"
    )
    branch = jnp.sum(pieces.astype(jnp.float32), axis=0)
    own = lax.dynamic_slice_in_dim(
        stream, lax.axis_index("cb") * (tokens // cb), tokens // cb, axis=0
    )
    updated = (own.astype(jnp.float32) + 0.5 * branch).astype(jnp.bfloat16)
    return sent_to_all(updated, "cb").reshape(stream.shape)


def per_device(
    residual,
    gain_first,
    gate_first,
    up_first,
    down_first,
    gain_second,
    gate_second,
    up_second,
    down_second,
):
    middle = half_step(residual, gain_first, gate_first, up_first, down_first)
    return half_step(middle, gain_second, gate_second, up_second, down_second)


def solution(mesh):
    in_specs = (
        P("grp", "ra"),
        P("ra"),
        P("ra", "cb"),
        P("ra", "cb"),
        P("cb", "ra"),
        P("ra"),
        P("ra", "cb"),
        P("ra", "cb"),
        P("cb", "ra"),
    )
    out_specs = P("grp", "ra")
    return jax.shard_map(
        per_device, mesh=mesh, in_specs=in_specs, out_specs=out_specs, check_vma=False
    )
```

time: 354 us -> 255 us (0.72)
  waiting for transfers between devices: 274 us -> 17.6 us
  blocking collectives: 45.3 us -> 208 us
  starting transfers between devices: 0.2 us -> 18.4 us
  between operations: 13.3 us -> 0.25 us
  other arithmetic: 11.1 us -> 2.72 us
    all_to_all x2 -> x6, blocking collectives: 45.3 us -> 208 us  [exchanged(): return lax.all_to_all(array, axis, 0, 0, tiled=True)]
    reduce_scatter x2 -> x0, waiting for transfers between devices: 162 us -> none  [in_one_piece(): out = lax.psum_scatter(both, axis, scatter_dimension=dim, tiled=True)]
    all_gather x2 -> x0, waiting for transfers between devices: 112 us -> none  [total_of_pieces(): return lax.all_gather(array, axis).sum(0)]
    all_to_all x0 -> x2, starting transfers between devices: none -> 18.4 us  [exchanged(): return lax.all_to_all(array, axis, 0, 0, tiled=True)]
    all_to_all x0 -> x2, waiting for transfers between devices: none -> 17.6 us  [exchanged(): return lax.all_to_all(array, axis, 0, 0, tiled=True)]
    reduce_sum x2 -> x4, other arithmetic: 5.01 us -> 0.27 us  [the longest x2 0.23 us: half_step(): total = jnp.sum(parts.astype(jnp.float32), axis=0)]
  transfers between devices with their start and end apart: 4 -> 2, of which waited for: 4 -> 2; matrix products, arithmetic and copies ran while one was open for 0% -> 0% of each run, Pallas kernels for 0% -> 0%
where the time goes in v1:
time: 255 us
  blocking collectives  208 us (82%)
  starting transfers between devices  18.4 us (7%)
  waiting for transfers between devices  17.6 us (7%)
  local copies, waits for them, and re-layouts  4.54 us (2%)
  matrix products  3.31 us (1%)
  other arithmetic  2.72 us (1%)
    all_to_all x6, blocking collectives, exchanged(): return lax.all_to_all(array, axis, 0, 0, tiled=True)  208 us
    all_to_all x2, starting transfers between devices, exchanged(): return lax.all_to_all(array, axis, 0, 0, tiled=True)  18.4 us
    all_to_all x2, waiting for transfers between devices, exchanged(): return lax.all_to_all(array, axis, 0, 0, tiled=True)  17.6 us
  transfers between devices with their start and end apart: 2, of which 2 were waited for; matrix products, arithmetic and copies ran while one was open for 0% of the time, Pallas kernels for 0%

profile of v1, /device:TPU:65, one launch (start us, length us, event | category | flops | bytes accessed | tf_op | source)
XLA Modules:
  0.0 254.8 jit_solution(2316688025666696381)
XLA Ops:
  0.0 0.7 convert_element_type.153
  0.7 1.0 fusion.1
  1.8 0.2 copy.47
  2.0 0.2 copy.46
  2.2 1.2 convolution_convert_fusion.2
  3.5 0.2 copy.45
  3.7 0.3 convolution_convert_fusion.3
  4.0 0.2 copy.44
  4.2 0.5 concatenate.21
  4.7 79.2 %all_to_all.40 = bf16[16,16,1536]{2,1,0:T(8,128)(2,1)S(1)} all-to-all(bf16[16,16,1536]{2,1,0:T(8,128)(2,1)S(1)} %concatenate.21), channel_id=1, replica_groups=mesh['grp'=2,'ra'=16,'cb'=16] {'ra'}, dimensions={0} | all-to-all | bytes 1572864 | tf_op jit(solution)/shard_map/all_to_all | solution.py:12
  84.0 0.2 fusion.15
  84.4 28.9 %all_to_all.41 = bf16[16,16,704]{2,1,0:T(8,128)(2,1)S(1)} all-to-all(bf16[16,16,704]{2,1,0:T(8,128)(2,1)S(1)} %broadcast_in_dim.8), channel_id=1, replica_groups=mesh['grp'=2,'ra'=16,'cb'=16] {'ra'}, dimensions={0} | all-to-all | bytes 720896 | tf_op jit(solution)/shard_map/all_to_all | solution.py:12
  113.3 0.9 convolution_convert_fusion.5
  114.2 14.7 %all-to-all-start.2 = ((bf16[16,16,256]{2,1,0:T(8,128)(2,1)}), bf16[16,16,256]{2,1,0:T(8,128)(2,1)S(1)}, u32[]{:S(2)}, u32[]{:S(2)}) async-start(bf16[16,16,256]{2,1,0:T(8,128)(2,1)} %bitcast.3), calls=%async_computation.2 | async-start | bytes 262144 | tf_op jit(solution)/shard_map/all_to_all | solution.py:12
  128.9 8.9 %all-to-all-done.2 = bf16[16,16,256]{2,1,0:T(8,128)(2,1)S(1)} async-done(((bf16[16,16,256]{2,1,0:T(8,128)(2,1)}), bf16[16,16,256]{2,1,0:T(8,128)(2,1)S(1)}, u32[]{:S(2)}, u32[]{:S(2)}) %all-to-all-start.2) | async-done | bytes 131104 | tf_op jit(solution)/shard_map/all_to_all | solution.py:12
  137.8 0.7 broadcast_in_dim.9
  138.5 3.7 %all-to-all-start.3 = ((bf16[16,16,256]{2,1,0:T(8,128)(2,1)}), bf16[16,16,256]{2,1,0:T(8,128)(2,1)S(1)}, u32[]{:S(2)}, u32[]{:S(2)}) async-start(bf16[16,16,256]{2,1,0:T(8,128)(2,1)} %broadcast_in_dim.9), calls=%async_computation.3 | async-start | bytes 262144 | tf_op jit(solution)/shard_map/all_to_all | solution.py:12
  142.2 8.7 %all-to-all-done.3 = bf16[16,16,256]{2,1,0:T(8,128)(2,1)S(1)} async-done(((bf16[16,16,256]{2,1,0:T(8,128)(2,1)}), bf16[16,16,256]{2,1,0:T(8,128)(2,1)S(1)}, u32[]{:S(2)}, u32[]{:S(2)}) %all-to-all-start.3) | async-done | bytes 131104 | tf_op jit(solution)/shard_map/all_to_all | solution.py:12
  151.1 0.2 copy.51
  151.3 0.2 copy.50
  151.5 0.3 convolution_convert_fusion
  151.7 0.2 copy.49
  151.9 0.5 copy-done.6
  152.4 0.3 convolution_convert_fusion.1
  152.9 0.5 concatenate.24
  153.4 44.2 %all_to_all.42 = bf16[16,16,1536]{2,1,0:T(8,128)(2,1)S(1)} all-to-all(bf16[16,16,1536]{2,1,0:T(8,128)(2,1)S(1)} %concatenate.24), channel_id=1, replica_groups=mesh['grp'=2,'ra'=16,'cb'=16] {'ra'}, dimensions={0} | all-to-all | bytes 1572864 | tf_op jit(solution)/shard_map/all_to_all | solution.py:12
  197.8 0.2 fusion.11
  198.1 25.4 %all_to_all.43 = bf16[16,16,704]{2,1,0:T(8,128)(2,1)S(1)} all-to-all(bf16[16,16,704]{2,1,0:T(8,128)(2,1)S(1)} %broadcast_in_dim.10), channel_id=1, replica_groups=mesh['grp'=2,'ra'=16,'cb'=16] {'ra'}, dimensions={0} | all-to-all | bytes 720896 | tf_op jit(solution)/shard_map/all_to_all | solution.py:12
  223.5 0.3 convolution_convert_fusion.4
  223.7 19.1 %all_to_all.44 = bf16[16,16,256]{2,1,0:T(8,128)(2,1)S(1)} all-to-all(bf16[16,16,256]{2,1,0:T(8,128)(2,1)S(1)} %bitcast.33), channel_id=1, replica_groups=mesh['grp'=2,'ra'=16,'cb'=16] {'cb'}, dimensions={0} | all-to-all | bytes 262144 | tf_op jit(solution)/shard_map/all_to_all | solution.py:12
  242.9 11.3 %all_to_all.45 = bf16[16,16,256]{2,1,0:T(8,128)(2,1)S(1)} all-to-all(bf16[16,16,256]{2,1,0:T(8,128)(2,1)S(1)} %broadcast_in_dim.11), channel_id=1, replica_groups=mesh['grp'=2,'ra'=16,'cb'=16] {'cb'}, dimensions={0} | all-to-all | bytes 262144 | tf_op jit(solution)/shard_map/all_to_all | solution.py:12
  254.2 0.7 copy.53
  (33 shorter events, 1.0 us)
Async XLA Ops:
  0.0 2.2 copy-start
  2.2 1.5 copy-start.1
  2.2 1.5 copy-start.4
  84.0 29.2 %copy-start.2 = (bf16[704,256]{1,0:T(8,128)(2,1)S(1)}, bf16[704,256]{1,0:T(8,128)(2,1)}, u32[]{:S(2)}) copy-start(bf16[704,256]{1,0:T(8,128)(2,1)} %param.13) | copy-start | bytes 1081348
  113.3 28.9 %copy-start.7 = (bf16[256]{0:T(256)(128)(2,1)S(1)}, bf16[256]{0:T(256)(128)(2,1)}, u32[]{:S(2)}) copy-start(bf16[256]{0:T(256)(128)(2,1)} %param.14) | copy-start | bytes 1540
  114.2 37.2 %copy-start.5 = (bf16[256,704]{0,1:T(8,128)(2,1)S(1)}, bf16[256,704]{0,1:T(8,128)(2,1)}, u32[]{:S(2)}) copy-start(bf16[256,704]{0,1:T(8,128)(2,1)} %param.16) | copy-start | bytes 1081348
  114.2 23.6 %all-to-all-start.2 = ((bf16[16,16,256]{2,1,0:T(8,128)(2,1)}), bf16[16,16,256]{2,1,0:T(8,128)(2,1)S(1)}, u32[]{:S(2)}, u32[]{:S(2)}) async-start(bf16[16,16,256]{2,1,0:T(8,128)(2,1)} %bitcast.3), calls=%async_computation.2 | async-start | bytes 262144 | tf_op jit(solution)/shard_map/all_to_all | solution.py:12
  138.5 12.4 %all-to-all-start.3 = ((bf16[16,16,256]{2,1,0:T(8,128)(2,1)}), bf16[16,16,256]{2,1,0:T(8,128)(2,1)S(1)}, u32[]{:S(2)}, u32[]{:S(2)}) async-start(bf16[16,16,256]{2,1,0:T(8,128)(2,1)} %broadcast_in_dim.9), calls=%async_computation.3 | async-start | bytes 262144 | tf_op jit(solution)/shard_map/all_to_all | solution.py:12
  151.5 1.0 copy-start.6
  197.8 25.7 %copy-start.3 = (bf16[704,256]{1,0:T(8,128)(2,1)S(1)}, bf16[704,256]{1,0:T(8,128)(2,1)}, u32[]{:S(2)}) copy-start(bf16[704,256]{1,0:T(8,128)(2,1)} %param.17) | copy-start | bytes 1081348
